TPU v7x, 512 devices: a whole 4x8x8 slice. The times are simulated.
512 devices in a mesh: ep: 32 (over z, x), tp: 16 (over y, core).
Axes of the slice: x: 4, y: 8, z: 8, core: 2. Of those that a mesh axis runs over, the one named last changes fastest.
Arguments:
- mix_rows: bfloat16 [8192, 2048], P('ep'), may hold values from -6 to 6
- mix_gain: bfloat16 [2048], replicated, may hold values from 0.099609375 to 1.8984375
- w_query: bfloat16 [1024, 2048], P('tp'), may hold values from -0.125 to 0.125
- w_key: bfloat16 [1024, 2048], P('tp'), may hold values from -0.125 to 0.125
- w_value: bfloat16 [1024, 2048], P('tp'), may hold values from -0.125 to 0.125
- key_offset: float32 [16, 8192], P('tp'), may hold values from -11 to 0
- w_out: bfloat16 [1024, 2048], P('tp'), may hold values from -0.1875 to 0.1875
- out_gain: bfloat16 [2048], replicated, may hold values from 0.099609375 to 1.8984375
- exp_rows: bfloat16 [3072, 2048], P('ep', 'tp'), may hold values from -100 to 100
- exp_gain: bfloat16 [2048], P('tp'), may hold values from 0.099609375 to 1.8984375
- routes: int32 [3072, 4], P('ep'), may hold values from 0 to 31, all different within a row; in each aligned block of 96 rows (0 to 95, 96 to 191, ...) at most 16 rows name the same one
- route_weight: float32 [3072, 4], P('ep'), may hold values from 0.05 to 1
- w_gate: bfloat16 [32, 2048, 2048], P('ep', None, 'tp'), may hold values from -0.5 to 0.5
- w_up: bfloat16 [32, 2048, 2048], P('ep', None, 'tp'), may hold values from -0.5 to 0.5
- w_down: bfloat16 [32, 2048, 2048], P('ep', 'tp'), may hold values from -0.1875 to 0.1875
Outputs:
- mix_out: bfloat16 [8192, 2048], P('ep')
- exp_out: bfloat16 [3072, 2048], P('ep', 'tp')
Inputs may be any that keep to these rules, and one draw needn't show every extreme that they name: `routes`: each row names 4 different experts. Within the rows of one device (aligned blocks of 96 rows) no expert is named by more than 16 rows, and in some blocks one expert is named by exactly 16 rows.
All inputs are finite; a program needn't handle non-finite values.
Results may differ from a plain program's by a relative error of at most 0.019.
Values may be sent and summed in bfloat16 or wider, within the bound.
No kernel may reach another device: no remote copies, remote signals or barrier semaphores. Data moves between devices by JAX's collectives and lax.ppermute only.
A program may use at most 128 MiB of HBM per device.

v0:
```python
import math
import jax
import jax.numpy as jnp
from jax import lax
from jax.sharding import Mesh
from jax.sharding import PartitionSpec as P

EP = ("ep_0", "ep_1")
TP = ("tp_0", "tp_1")
EPSILON = 1e-06
CLAMP_LIMIT = 7.0
SILU_SHARPNESS = 1.702


def gathered_by_axis(value, axes, dim):
    out = value
    for number in range(len(axes) - 1, -1, -1):
        out = lax.all_gather(out, axes[number], axis=dim, tiled=True)
    return out


def split_up(value, dim, devices):
    dims = value.shape
    tiles = value.reshape(*dims[:dim], devices, dims[dim] // devices, *dims[dim + 1 :])
    return jnp.moveaxis(tiles, dim, 0)


def sent_and_summed(value, axis, dim):
    devices = lax.axis_size(axis)
    tiles = lax.all_to_all(split_up(value, dim, devices), axis, 0, 0, tiled=True)
    return jnp.sum(tiles.astype(jnp.float32), axis=0)


def from_everyone(value, axis):
    copies = jnp.broadcast_to(value, (lax.axis_size(axis), *value.shape))
    return lax.all_to_all(copies, axis, split_axis=0, concat_axis=0, tiled=True)


def of_everyone(value, axis):
    return from_everyone(value, axis).sum(axis=0)


def gather_turned(arrays, axis, dims):
    turned = [jnp.moveaxis(a, dim, 0) for a, dim in zip(arrays, dims)]
    widths = [t[0].size for t in turned]
    both = jnp.concatenate([t.reshape(-1, w) for t, w in zip(turned, widths)], axis=1)
    out = lax.all_gather(both, axis, axis=0, tiled=True)
    tiles = jnp.split(out, [sum(widths[:k]) for k in range(1, len(widths))], axis=1)
    return tuple(
        (
            jnp.moveaxis(b.reshape(-1, *t.shape[1:]), 0, dim)
            for b, t, dim in zip(tiles, turned, dims)
        )
    )


def summed_rows_2(value, chips, core, dim):
    sizes = (lax.axis_size(chips), lax.axis_size(core))
    tiles = split_up(value, dim, sizes[0] * sizes[1])
    inside = tiles.shape[1:]
    tiles = tiles.reshape(*sizes, *inside).swapaxes(0, 1).reshape(-1, *inside)
    tiles = lax.psum_scatter(tiles, core, scatter_dimension=0, tiled=True)
    return lax.psum_scatter(tiles, chips, scatter_dimension=0, tiled=True)[0]


def normalize(numbers, gain):
    factor = lax.rsqrt(jnp.mean(numbers * numbers, axis=-1, keepdims=True) + EPSILON)
    return numbers * factor * gain.astype(jnp.float32)


def project(normed, weight):
    product = lax.dot_general(
        normed, weight, (((1,), (1,)), ((), ())), preferred_element_type=jnp.float32
    )
    return product.astype(jnp.bfloat16)


def gated_units(gate_pre, up_pre):
    gate_part = jnp.minimum(gate_pre, CLAMP_LIMIT)
    up_part = jnp.clip(up_pre, -CLAMP_LIMIT, CLAMP_LIMIT)
    return (up_part + 1.0) * (gate_part * jax.nn.sigmoid(SILU_SHARPNESS * gate_part))


def stick_terms(queries, block_pairs, offset_values, query_index, key_index):
    heads_here = queries.shape[1]
    head_size = queries.shape[2]
    width = heads_here * head_size
    key_rows = block_pairs[:, :width].reshape(-1, heads_here, head_size)
    value_rows = block_pairs[:, width:].reshape(-1, heads_here, head_size)
    scores = jnp.einsum(
        "thd,shd->hts", queries, key_rows, preferred_element_type=jnp.float32
    ) / math.sqrt(head_size)
    scores = scores + offset_values[:, None, :]
    visible = (key_index[None, :] < query_index[:, None])[None]
    keep_log = jnp.where(visible, jax.nn.log_sigmoid(-scores), 0.0)
    later_sum = lax.cumsum(keep_log, axis=2, reverse=True) - keep_log
    exponent = jax.nn.log_sigmoid(scores) + later_sum
    weights = jnp.where(visible, jnp.exp(exponent), 0.0).astype(jnp.bfloat16)
    attended = jnp.einsum("hts,shd->thd", weights, value_rows, preferred_element_type=jnp.float32)
    return (attended, jnp.sum(keep_log, axis=2))


def on_device(
    mix_rows,
    mix_gain,
    w_query,
    w_key,
    w_value,
    key_offset,
    w_out,
    out_gain,
    exp_rows,
    exp_gain,
    routes,
    route_weight,
    w_gate,
    w_up,
    w_down,
):
    row_count = mix_rows.shape[0]
    heads_here = key_offset.shape[0]
    head_size = w_query.shape[0] // heads_here
    normed = normalize(mix_rows.astype(jnp.float32), mix_gain).astype(jnp.bfloat16)
    queries = project(normed, w_query).reshape(row_count, heads_here, head_size)
    own_pairs = jnp.concatenate([project(normed, w_key), project(normed, w_value)], axis=1)
    own_start = lax.axis_index(EP) * row_count
    query_index = own_start + jnp.arange(row_count, dtype=jnp.int32)
    every_pair = gathered_by_axis(own_pairs, EP, 0)
    key_index = jnp.arange(every_pair.shape[0], dtype=jnp.int32)
    attended, _ = stick_terms(queries, every_pair, key_offset, query_index, key_index)
    attended = attended.reshape(row_count, heads_here * head_size).astype(jnp.bfloat16)
    tp_count = lax.axis_size(TP)
    model_width = w_out.shape[1]
    column_count = model_width // tp_count
    columns = w_out
    share = sent_and_summed(
        lax.dot_general(
            columns, attended, (((0,), (1,)), ((), ())), preferred_element_type=jnp.float32
        ).astype(jnp.bfloat16),
        TP,
        0,
    )
    row_sums = of_everyone(jnp.sum(share * share, axis=0), TP)
    factor = lax.rsqrt(row_sums / model_width + EPSILON)
    gain_share = lax.dynamic_slice_in_dim(
        out_gain, lax.axis_index(TP) * column_count, column_count, 0
    ).astype(jnp.float32)
    own_columns = (share.T * factor[:, None] * gain_share[None, :]).astype(jnp.bfloat16)
    mix_out = lax.all_gather(own_columns, TP, axis=1, tiled=True)
    token_count, top_count = routes.shape
    ep_count = lax.axis_size(EP)
    experts = w_gate.shape[0] * ep_count
    capacity = 4 * token_count * top_count // (3 * experts)
    route_list = routes.reshape(-1)
    matches = (route_list[:, None] == jnp.arange(experts, dtype=jnp.int32)[None, :]).astype(
        jnp.int32
    )
    earlier = jnp.cumsum(matches, axis=0) - matches
    slot_index = route_list * capacity + jnp.sum(earlier * matches, axis=1)
    token_of = jnp.arange(route_list.shape[0], dtype=jnp.int32) // top_count + 1
    owners = jnp.zeros((experts * capacity,), jnp.int32).at[slot_index].set(token_of)
    whole_rows, whole_gain = gather_turned((exp_rows, exp_gain), TP, (1, 0))
    normed_exp = normalize(whole_rows.astype(jnp.float32), whole_gain).astype(jnp.bfloat16)
    outgoing = jnp.where(
        owners[:, None] > 0, normed_exp[jnp.maximum(owners - 1, 0)], jnp.zeros((), jnp.bfloat16)
    )
    arrived = lax.all_to_all(outgoing, EP, split_axis=0, concat_axis=0, tiled=True)
    gate_pre = jnp.dot(arrived, w_gate[0], preferred_element_type=jnp.float32)
    up_pre = jnp.dot(arrived, w_up[0], preferred_element_type=jnp.float32)
    hidden = gated_units(gate_pre, up_pre).astype(jnp.bfloat16)
    columns = w_down[0]
    expert_out = (
        summed_rows_2(
            lax.dot_general(
                columns, hidden, (((0,), (1,)), ((), ())), preferred_element_type=jnp.float32
            ).astype(jnp.bfloat16),
            "tp_0",
            "tp_1",
            0,
        )
        .astype(jnp.float32)
        .astype(jnp.bfloat16)
    )
    returned = lax.all_to_all(expert_out, EP, split_axis=1, concat_axis=1, tiled=True)
    picked = (
        jnp.take(returned, slot_index, axis=1)
        .astype(jnp.float32)
        .reshape(-1, token_count, top_count)
    )
    combined = jnp.sum(picked * route_weight[None], axis=2)
    exp_out = combined.T.astype(jnp.bfloat16)
    return (mix_out, exp_out)


def solution(mesh):
    torus = Mesh(mesh.devices.reshape(8, 4, 8, 2), ("ep_0", "ep_1", "tp_0", "tp_1"))
    in_specs = (
        P(EP, None),
        P(),
        P(TP, None),
        P(TP, None),
        P(TP, None),
        P(TP, None),
        P(TP, None),
        P(),
        P(EP, TP),
        P(TP),
        P(EP, None),
        P(EP, None),
        P(EP, None, TP),
        P(EP, None, TP),
        P(EP, TP, None),
    )
    out_specs = (P(EP, None), P(EP, TP))
    return jax.shard_map(
        on_device, mesh=torus, in_specs=in_specs, out_specs=out_specs, check_vma=False
    )
```

profile of v0, /device:TPU:1, one launch (start us, length us, event | category | flops | bytes accessed | tf_op | source)
XLA Modules:
  0.0 288.5 jit_solution(9969811278149230020)
XLA Ops:
  8.1 1.6 fusion.13
  9.6 0.7 convert_element_type.101
  10.3 1.8 convolution_convert_fusion.3
  12.1 1.8 convolution_convert_fusion.4
  13.9 11.3 %all_gather.12 = bf16[1024,128]{0,1:T(8,128)(2,1)} all-gather(bf16[256,128]{0,1:T(8,128)(2,1)S(1)} %pad_maximum_fusion), channel_id=1, replica_groups=mesh['ep_0'=8,'ep_1'=4,'tp_0'=8,'tp_1'=2] {'ep_1'}, dimensions={0}, use_global_device_ids=true | all-gather | bytes 327680 | tf_op jit(solution)/shard_map/all_gather | solution.py:18
  25.2 0.7 broadcast_multiply_fusion
  25.9 0.8 copy.81
  27.1 0.9 reduce-window.16
  28.4 2.9 %scatter_custom_fusion = s32[512]{0:T(512)S(1)} fusion(s32[384]{0:T(512)S(1)} %fusion.55, s32[384]{0:T(512)S(1)} %fusion.51, s32[]{:T(128)} %constant.94.clone.1), kind=kCustom, calls=%fused_computation.97 | custom fusion | bytes 2052 | tf_op jit(solution)/shard_map/scatter | solution.py:161
  31.3 0.8 pad_maximum_fusion.1
  32.1 23.8 %all_gather.15 = bf16[2048,97]{0,1:T(8,128)(2,1)S(1)} all-gather(bf16[128,97]{0,1:T(8,128)(2,1)S(1)} %pad_maximum_fusion.1), channel_id=1, replica_groups=mesh['ep_0'=8,'ep_1'=4,'tp_0'=8,'tp_1'=2] {'tp_0','tp_1'}, dimensions={0}, use_global_device_ids=true | all-gather | bytes 422144 | tf_op jit(solution)/shard_map/all_gather | solution.py:47
  56.3 2.5 gather_fusion
  58.8 1.5 broadcast_select_fusion
  60.3 10.9 %all-to-all-start.2 = ((bf16[32,16,2048]{2,1,0:T(8,128)(2,1)}), bf16[32,16,2048]{2,1,0:T(8,128)(2,1)S(1)}, u32[]{:S(2)}, u32[]{:S(2)}) async-start(bf16[32,16,2048]{2,1,0:T(8,128)(2,1)} %broadcast_select_fusion), calls=%async_computation.2 | async-start | bytes 4194304 | tf_op jit(solution)/shard_map/all_to_all | solution.py:167
  71.2 0.5 reduce-scatter.3.cloned.1.call-start
  71.7 0.6 all-gather.3.cloned.1.call-done
  72.3 7.1 %fusion = f32[256,8192]{1,0:T(8,128)} fusion(f32[8192]{0:T(1024)S(1)} %bitcast.114, bf16[64,2048]{1,0:T(8,128)(2,1)S(1)} %copy-done.5, bf16[8192,128]{0,1:T(8,128)(2,1)} %all-gather.3.cloned.1.call-done, bf16[256,2048]{1,0:T(8,128)(2,1)} %param.15, f32[2048]{0:T(1024)S(1)} %convert_element_type.101, f32[256]{0:T(256)S(1)} %add_rsqrt_fusion.1), kind=kOutput, calls=%fused_computation.6 | convolution fusion | flops 341852160 | bytes 10789888 | tf_op jit(solution)/shard_map/thd,shd->hts/dot_general | solution.py:90
  79.4 7.4 %fusion.9 = f32[32,8,64,128]{3,1,2,0:T(8,128)S(1)} fusion(f32[256,8192]{1,0:T(8,128)} %fusion, s32[256]{0:T(256)S(1)} %iota_add_fusion), kind=kLoop, calls=%fused_computation.17 | loop fusion | flops 18874368 | bytes 16778240
  86.8 4.8 %copy.93 = f32[32,8,64,128]{3,2,1,0:T(8,128)} copy(f32[32,8,64,128]{3,1,2,0:T(8,128)S(1)} %fusion.9) | data formatting | bytes 16777216
  91.7 9.3 %copy.76 = f32[1,256,64,128]{1,2,3,0:T(8,128)} copy(f32[1,256,64,128]{3,2,1,0:T(8,128)} %bitcast.105) | data formatting | bytes 16777216 | tf_op jit(solution)/shard_map/reshape
  101.0 20.7 %all-to-all-done.2 = bf16[32,16,2048]{2,1,0:T(8,128)(2,1)S(1)} async-done(((bf16[32,16,2048]{2,1,0:T(8,128)(2,1)}), bf16[32,16,2048]{2,1,0:T(8,128)(2,1)S(1)}, u32[]{:S(2)}, u32[]{:S(2)}) %all-to-all-start.2) | async-done | bytes 2097184 | tf_op jit(solution)/shard_map/all_to_all | solution.py:167
  121.6 0.7 convolution_minimum_fusion
  122.3 4.7 %fusion.12 = bf16[2048,512]{0,1:T(8,128)(2,1)} fusion(bf16[512,2048]{1,0:T(8,128)(2,1)S(1)} %bitcast.107, bf16[1,128,2048]{2,1,0:T(8,128)(2,1)S(1)} %copy-done, bf16[1,2048,128]{2,1,0:T(8,128)(2,1)} %param.28, f32[512,128]{1,0:T(8,128)S(1)} %convolution_minimum_fusion), kind=kOutput, calls=%fused_computation.20 | convolution fusion | flops 538509312 | bytes 5505024 | tf_op jit(solution)/shard_map/dot_general | solution.py:174
  127.0 3.2 %reshape_reshape.3 = bf16[8,2,128,512]{2,1,0,3:T(2,128)(2,1)S(1)} reshape(bf16[2048,512]{0,1:T(8,128)(2,1)} %fusion.12) | data formatting | bytes 4194304 | tf_op jit(solution)/shard_map/reshape;reshape | solution.py:61
  130.3 4.7 %copy.87 = bf16[8,2,128,512]{3,2,0,1:T(8,128)(2,1)} copy(bf16[8,2,128,512]{2,1,0,3:T(2,128)(2,1)S(1)} %reshape_reshape.3) | data formatting | bytes 4194304 | tf_op jit(solution)/shard_map/reshape;reshape | solution.py:61
  135.1 24.0 %fusion.67 = f32[1,256,64,128]{1,2,3,0:T(8,128)} fusion(f32[1,256,64,128]{1,2,3,0:T(8,128)} %copy.76), kind=kOutput, calls=%fused_computation.110 | output fusion | flops 266338304 | bytes 16777216 | tf_op jit(solution)/shard_map/reduce-window
  159.1 9.0 %copy.77 = f32[1,256,64,128]{3,2,1,0:T(8,128)} copy(f32[1,256,64,128]{1,2,3,0:T(8,128)} %fusion.67) | data formatting | bytes 16777216 | tf_op jit(solution)/shard_map/reduce-window
  168.1 0.8 slice_bitcast_fusion.1
  169.0 0.6 reduce-window.15
  169.7 2.3 broadcast.140
  172.0 1.0 copy-done.2
  173.0 18.7 %fusion.23 = bf16[256,64]{0,1:T(8,128)(2,1)S(1)} fusion(f32[32,8,64,128]{3,2,1,0:T(8,128)S(1)} %bitcast.110, f32[32,8,64,128]{3,2,1,0:T(8,128)S(1)} %bitcast.109, f32[256,8192]{1,0:T(8,128)} %fusion, s32[256]{0:T(256)S(1)} %iota_add_fusion, bf16[8192,128]{0,1:T(8,128)(2,1)S(1)} %copy-done.3), kind=kOutput, calls=%fused_computation.39 | convolution fusion | flops 314589184 | bytes 26248192 | tf_op jit(solution)/shard_map/hts,shd->thd/dot_general | solution.py:99
  191.8 0.5 fusion.16
  192.3 1.2 copy.110
  193.5 6.5 %all-to-all-start = ((bf16[16,128,256]{1,2,0:T(8,128)(2,1)}), bf16[16,128,256]{1,2,0:T(8,128)(2,1)S(1)}, u32[]{:S(2)}, u32[]{:S(2)}) async-start(bf16[16,128,256]{1,2,0:T(8,128)(2,1)} %bitcast.102), calls=%async_computation | async-start | bytes 2097152 | tf_op jit(solution)/shard_map/all_to_all | solution.py:30
  200.1 0.5 reduce-scatter.5.cloned.1.call-update
  200.6 30.3 %all-to-all-done = bf16[16,128,256]{1,2,0:T(8,128)(2,1)S(1)} async-done(((bf16[16,128,256]{1,2,0:T(8,128)(2,1)}), bf16[16,128,256]{1,2,0:T(8,128)(2,1)S(1)}, u32[]{:S(2)}, u32[]{:S(2)}) %all-to-all-start) | async-done | bytes 1048608 | tf_op jit(solution)/shard_map/all_to_all | solution.py:30
  231.2 0.6 broadcast_in_dim.31
  231.8 4.2 %all-to-all-start.1 = ((f32[16,1,256]{2,1,0:T(1,128)}), f32[16,1,256]{2,1,0:T(1,128)S(1)}, u32[]{:S(2)}, u32[]{:S(2)}) async-start(f32[16,1,256]{2,1,0:T(1,128)} %broadcast_in_dim.31), calls=%async_computation.1 | async-start | bytes 32768 | tf_op jit(solution)/shard_map/all_to_all | solution.py:36
  236.0 0.8 dynamic-slice_convert_fusion
  236.8 6.6 %all-to-all-done.1 = f32[16,1,256]{2,1,0:T(1,128)S(1)} async-done(((f32[16,1,256]{2,1,0:T(1,128)}), f32[16,1,256]{2,1,0:T(1,128)S(1)}, u32[]{:S(2)}, u32[]{:S(2)}) %all-to-all-start.1) | async-done | bytes 16416 | tf_op jit(solution)/shard_map/all_to_all | solution.py:36
  243.4 0.7 fusion.46
  244.3 1.7 copy.88
  246.0 6.3 %all-to-all-start.3 = ((bf16[128,32,16]{0,2,1:T(8,128)(2,1)}), bf16[128,32,16]{0,2,1:T(8,128)(2,1)S(1)}, u32[]{:S(2)}, u32[]{:S(2)}) async-start(bf16[128,32,16]{0,2,1:T(8,128)(2,1)} %bitcast.21), calls=%async_computation.5 | async-start | bytes 262144 | tf_op jit(solution)/shard_map/all_to_all | solution.py:184
  252.7 23.3 %all-gather.5.cloned.1.call-done = bf16[256,2048]{1,0:T(8,128)(2,1)} async-done(((bf16[256,128]{1,0:T(8,128)(2,1)}), bf16[256,2048]{1,0:T(8,128)(2,1)}) %all-gather.5.cloned.1.call-update) | async-done | bytes 1048592 | tf_op jit(solution)/shard_map/all_gather | solution.py:149
  276.0 1.4 gather_fusion.1
  277.4 0.9 multiply_reduce_fusion
  278.4 2.3 copy.112
  (61 shorter events, 2.3 us)
Async XLA Ops:
  8.0 114.3 %copy-start = (bf16[1,128,2048]{2,1,0:T(8,128)(2,1)S(1)}, bf16[1,128,2048]{2,1,0:T(8,128)(2,1)}, u32[]{:S(2)}) copy-start(bf16[1,128,2048]{2,1,0:T(8,128)(2,1)} %param.29) | copy-start | bytes 1572868
  8.0 64.3 %all-gather.3.cloned.1.call-start = ((), (), s32[]{:S(2)}) async-start(), calls=%async_computation.6 | async-start | bytes 2359296 | tf_op jit(solution)/shard_map/all_gather | solution.py:18
  58.8 13.5 %copy-start.5 = (bf16[64,2048]{1,0:T(8,128)(2,1)S(1)}, bf16[64,2048]{1,0:T(8,128)(2,1)}, u32[]{:S(2)}) copy-start(bf16[64,2048]{1,0:T(8,128)(2,1)} %param.17) | copy-start | bytes 786436
  58.8 13.5 %copy-start.7 = (f32[1,8192]{1,0:T(1,128)S(1)}, f32[1,8192]{1,0:T(1,128)}, u32[]{:S(2)}) copy-start(f32[1,8192]{1,0:T(1,128)} %param.20) | copy-start | bytes 98308
  60.3 61.3 %all-to-all-start.2 = ((bf16[32,16,2048]{2,1,0:T(8,128)(2,1)}), bf16[32,16,2048]{2,1,0:T(8,128)(2,1)S(1)}, u32[]{:S(2)}, u32[]{:S(2)}) async-start(bf16[32,16,2048]{2,1,0:T(8,128)(2,1)} %broadcast_select_fusion), calls=%async_computation.2 | async-start | bytes 4194304 | tf_op jit(solution)/shard_map/all_to_all | solution.py:167
  71.2 128.9 %reduce-scatter.3.cloned.1.call-start = ((), (), s32[]{:S(2)}) async-start(), calls=%async_computation.8 | async-start | bytes 3145728 | tf_op jit(solution)/shard_map/reduce_scatter | solution.py:62
  91.7 29.9 %copy-start.4 = (bf16[1,2048,128]{2,1,0:T(8,128)(2,1)S(1)}, bf16[1,2048,128]{2,1,0:T(8,128)(2,1)}, u32[]{:S(2)}) copy-start(bf16[1,2048,128]{2,1,0:T(8,128)(2,1)} %param.27) | copy-start | bytes 1572868
  159.1 12.9 %copy-start.3 = (bf16[8192,128]{0,1:T(8,128)(2,1)S(1)}, bf16[8192,128]{0,1:T(8,128)(2,1)}, u32[]{:S(2)}) copy-start(bf16[8192,128]{0,1:T(8,128)(2,1)} %all-gather.3.cloned.1.call-done) | copy-start | bytes 6291460
  169.6 3.4 %copy-start.2 = (f32[1,256,64,128]{3,2,1,0:T(8,128)S(1)}, f32[1,256,64,128]{3,2,1,0:T(8,128)}, u32[]{:S(2)}) copy-start(f32[1,256,64,128]{3,2,1,0:T(8,128)} %copy.77) | copy-start | bytes 25165828
  173.0 18.7 %copy-start.6 = (bf16[64,2048]{1,0:T(8,128)(2,1)S(1)}, bf16[64,2048]{1,0:T(8,128)(2,1)}, u32[]{:S(2)}) copy-start(bf16[64,2048]{1,0:T(8,128)(2,1)} %param.21) | copy-start | bytes 786436
  173.0 107.6 %copy-start.1 = (bf16[1,128,2048]{2,1,0:T(8,128)(2,1)S(1)}, bf16[1,128,2048]{2,1,0:T(8,128)(2,1)}, u32[]{:S(2)}) copy-start(bf16[1,128,2048]{2,1,0:T(8,128)(2,1)} %param.29) | copy-start | bytes 1572868
  191.8 60.6 %copy-start.8 = (s32[96,4]{0,1:T(4,128)S(1)}, s32[96,4]{0,1:T(4,128)}, u32[]{:S(2)}) copy-start(s32[96,4]{0,1:T(4,128)} %param.25) | copy-start | bytes 4612
  191.8 60.7 %copy-start.9 = (f32[96,4]{0,1:T(4,128)S(1)}, f32[96,4]{0,1:T(4,128)}, u32[]{:S(2)}) copy-start(f32[96,4]{0,1:T(4,128)} %param.26) | copy-start | bytes 4612
  193.5 37.4 %all-to-all-start = ((bf16[16,128,256]{1,2,0:T(8,128)(2,1)}), bf16[16,128,256]{1,2,0:T(8,128)(2,1)S(1)}, u32[]{:S(2)}, u32[]{:S(2)}) async-start(bf16[16,128,256]{1,2,0:T(8,128)(2,1)} %bitcast.102), calls=%async_computation | async-start | bytes 2097152 | tf_op jit(solution)/shard_map/all_to_all | solution.py:30
  200.0 44.4 %reduce-scatter.5.cloned.1.call-start = ((), (), s32[]{:S(2)}) async-start(), calls=%async_computation.9 | async-start | bytes 1179648 | tf_op jit(solution)/shard_map/reduce_scatter | solution.py:63
  231.8 11.6 %all-to-all-start.1 = ((f32[16,1,256]{2,1,0:T(1,128)}), f32[16,1,256]{2,1,0:T(1,128)S(1)}, u32[]{:S(2)}, u32[]{:S(2)}) async-start(f32[16,1,256]{2,1,0:T(1,128)} %broadcast_in_dim.31), calls=%async_computation.1 | async-start | bytes 32768 | tf_op jit(solution)/shard_map/all_to_all | solution.py:36
  236.0 40.0 %all-gather.5.cloned.1.call-start = ((), (), s32[]{:S(2)}) async-start(), calls=%async_computation.7 | async-start | bytes 1114112 | tf_op jit(solution)/shard_map/all_gather | solution.py:149
  246.0 30.0 %all-to-all-start.3 = ((bf16[128,32,16]{0,2,1:T(8,128)(2,1)}), bf16[128,32,16]{0,2,1:T(8,128)(2,1)S(1)}, u32[]{:S(2)}, u32[]{:S(2)}) async-start(bf16[128,32,16]{0,2,1:T(8,128)(2,1)} %bitcast.21), calls=%async_computation.5 | async-start | bytes 262144 | tf_op jit(solution)/shard_map/all_to_all | solution.py:184
Sparse Core Ops, SparseCore 0:
  25.3 46.9 all-gather.2
  244.3 31.6 all-gather.4
Sparse Core Ops, SparseCore 1:
  135.1 14.9 reduce-scatter.2
  203.3 40.1 reduce-scatter.4
where the time goes:
time: 294 us; the launch traced here: 289 us
  waiting for transfers between devices  82.1 us (28%)
  local copies, waits for them, and re-layouts  50 us (17%)
  other arithmetic  41.4 us (14%)
  matrix products  35.2 us (12%)
  blocking collectives  35 us (12%)
  starting transfers between devices  28.5 us (10%)
  between operations  16.3 us (6%)
    all_to_all x1, waiting for transfers between devices, sent_and_summed(): lax.all_to_all(split_up(value, dim, devices), axis, 0, 0, tiled=True)  30.3 us
    another operation x4, other arithmetic  25.5 us
    all_gather x1, blocking collectives, gather_turned(): out = lax.all_gather(both, axis, axis=0, tiled=True)  23.8 us
    all_gather x1, waiting for transfers between devices, on_device(): mix_out = lax.all_gather(own_columns, TP, axis=1, tiled=True)  23.3 us
    all_to_all x1, waiting for transfers between devices, on_device(): lax.all_to_all(outgoing, EP, split_axis=0, concat_axis=0, tiled=True)  20.7 us
    dot_general x1, matrix products, stick_terms(): jnp.einsum('hts,shd->thd', weights, value_rows, preferred_element_type=jn...  18.7 us
    another operation x6, local copies, waits for them, and re-layouts  12.5 us
    all_gather x1, blocking collectives, gathered_by_axis(): out = lax.all_gather(out, axes[number], axis=dim, tiled=True)  11.3 us
  transfers between devices with their start and end apart: 8, of which 5 were waited for; matrix products, arithmetic and copies ran while one was open for 35% of the time, Pallas kernels for 0%

commit v1 on v0

--- a/solution.py
+++ b/solution.py
@@ -146,7 +146,8 @@
         out_gain, lax.axis_index(TP) * column_count, column_count, 0
     ).astype(jnp.float32)
     own_columns = (share.T * factor[:, None] * gain_share[None, :]).astype(jnp.bfloat16)
-    mix_out = lax.all_gather(own_columns, TP, axis=1, tiled=True)
+    repeated = jnp.stack([own_columns] * lax.axis_size(TP))
+    mix_out = jnp.concatenate(lax.all_to_all(repeated, TP, 0, 0), axis=1)
     token_count, top_count = routes.shape
     ep_count = lax.axis_size(EP)
     experts = w_gate.shape[0] * ep_count

time: 294 us -> 314 us (1.068)
  the two profiles are of different devices: /device:TPU:1 before, /device:TPU:16 now
where the time goes in v1:
time: 314 us; the launch traced here: 308 us
  waiting for transfers between devices  91.9 us (29%)
  local copies, waits for them, and re-layouts  50 us (16%)
  starting transfers between devices  42.8 us (14%)
  other arithmetic  40.7 us (13%)
  matrix products  35.6 us (11%)
  blocking collectives  31.4 us (10%)
  between operations  16.1 us (5%)
    reduce_scatter x1, waiting for transfers between devices, summed_rows_2(): return lax.psum_scatter(tiles, chips, scatter_dimension=0, tiled=True)[0]  41.2 us
    another operation x4, other arithmetic  25.5 us
    all_to_all x1, waiting for transfers between devices, sent_and_summed(): lax.all_to_all(split_up(value, dim, devices), axis, 0, 0, tiled=True)  24.4 us
    dot_general x1, matrix products, stick_terms(): jnp.einsum('hts,shd->thd', weights, value_rows, preferred_element_type=jn...  19.1 us
    all_gather x1, blocking collectives, gather_turned(): out = lax.all_gather(both, axis, axis=0, tiled=True)  18 us
    all_gather x1, blocking collectives, gathered_by_axis(): out = lax.all_gather(out, axes[number], axis=dim, tiled=True)  13.3 us
    all_gather x1, waiting for transfers between devices, gathered_by_axis(): out = lax.all_gather(out, axes[number], axis=dim, tiled=True)  13.3 us
    another operation x6, local copies, waits for them, and re-layouts  12.4 us
  transfers between devices with their start and end apart: 8, of which 5 were waited for; matrix products, arithmetic and copies ran while one was open for 34% of the time, Pallas kernels for 0%

profile of v1, /device:TPU:16, one launch (start us, length us, event | category | flops | bytes accessed | tf_op | source)
XLA Modules:
  0.0 308.5 jit_solution(14282704694856980478)
XLA Ops:
  8.1 1.6 fusion.13
  9.6 0.7 convert_element_type.101
  10.3 1.8 convolution_convert_fusion.3
  12.1 1.8 convolution_convert_fusion.4
  13.9 13.3 %all_gather.9 = bf16[1024,128]{0,1:T(8,128)(2,1)} all-gather(bf16[256,128]{0,1:T(8,128)(2,1)S(1)} %pad_maximum_fusion), channel_id=1, replica_groups=mesh['ep_0'=8,'ep_1'=4,'tp_0'=8,'tp_1'=2] {'ep_1'}, dimensions={0}, use_global_device_ids=true | all-gather | bytes 327680 | tf_op jit(solution)/shard_map/all_gather | solution.py:18
  27.3 0.7 broadcast_multiply_fusion
  27.9 0.8 copy.99
  29.2 0.9 reduce-window.16
  30.4 2.9 scatter_custom_fusion
  33.5 0.8 pad_maximum_fusion.1
  34.3 18.0 %all_gather.11 = bf16[2048,97]{0,1:T(8,128)(2,1)S(1)} all-gather(bf16[128,97]{0,1:T(8,128)(2,1)S(1)} %pad_maximum_fusion.1), channel_id=1, replica_groups=mesh['ep_0'=8,'ep_1'=4,'tp_0'=8,'tp_1'=2] {'tp_0','tp_1'}, dimensions={0}, use_global_device_ids=true | all-gather | bytes 422144 | tf_op jit(solution)/shard_map/all_gather | solution.py:47
  52.6 2.5 gather_fusion
  55.1 1.5 broadcast_select_fusion
  56.6 11.2 %all-to-all-start.3 = ((bf16[32,16,2048]{2,1,0:T(8,128)(2,1)}), bf16[32,16,2048]{2,1,0:T(8,128)(2,1)S(1)}, u32[]{:S(2)}, u32[]{:S(2)}) async-start(bf16[32,16,2048]{2,1,0:T(8,128)(2,1)} %broadcast_select_fusion), calls=%async_computation.3 | async-start | bytes 4194304 | tf_op jit(solution)/shard_map/all_to_all | solution.py:168
  67.8 0.3 reduce-scatter.3.cloned.1.call-start
  68.2 13.3 %all-gather.2.cloned.1.call-done = bf16[8192,128]{0,1:T(8,128)(2,1)} async-done(((bf16[1024,128]{0,1:T(8,128)(2,1)}), bf16[8192,128]{0,1:T(8,128)(2,1)}) %all-gather.2.cloned.1.call-update) | async-done | bytes 2097168 | tf_op jit(solution)/shard_map/all_gather | solution.py:18
  81.5 7.1 %fusion = f32[256,8192]{1,0:T(8,128)} fusion(f32[8192]{0:T(1024)S(1)} %bitcast.118, bf16[64,2048]{1,0:T(8,128)(2,1)S(1)} %copy-done.3, bf16[8192,128]{0,1:T(8,128)(2,1)} %all-gather.2.cloned.1.call-done, bf16[256,2048]{1,0:T(8,128)(2,1)} %param.15, f32[2048]{0:T(1024)S(1)} %convert_element_type.101, f32[256]{0:T(256)S(1)} %add_rsqrt_fusion.1), kind=kOutput, calls=%fused_computation.6 | convolution fusion | flops 341852160 | bytes 10789888 | tf_op jit(solution)/shard_map/thd,shd->hts/dot_general | solution.py:90
  88.6 7.4 %fusion.9 = f32[32,8,64,128]{3,1,2,0:T(8,128)S(1)} fusion(f32[256,8192]{1,0:T(8,128)} %fusion, s32[256]{0:T(256)S(1)} %iota_add_fusion), kind=kLoop, calls=%fused_computation.17 | loop fusion | flops 18874368 | bytes 16778240
  96.0 4.8 %copy.112 = f32[32,8,64,128]{3,2,1,0:T(8,128)} copy(f32[32,8,64,128]{3,1,2,0:T(8,128)S(1)} %fusion.9) | data formatting | bytes 16777216
  100.9 9.7 %copy.93 = f32[1,256,64,128]{1,2,3,0:T(8,128)} copy(f32[1,256,64,128]{3,2,1,0:T(8,128)} %bitcast.108) | data formatting | bytes 16777216 | tf_op jit(solution)/shard_map/reshape
  110.6 24.0 %fusion.67 = f32[1,256,64,128]{1,2,3,0:T(8,128)} fusion(f32[1,256,64,128]{1,2,3,0:T(8,128)} %copy.93), kind=kOutput, calls=%fused_computation.110 | output fusion | flops 266338304 | bytes 16777216 | tf_op jit(solution)/shard_map/reduce-window
  134.6 8.9 %copy.94 = f32[1,256,64,128]{3,2,1,0:T(8,128)} copy(f32[1,256,64,128]{1,2,3,0:T(8,128)} %fusion.67) | data formatting | bytes 16777216 | tf_op jit(solution)/shard_map/reduce-window
  143.5 0.8 slice_bitcast_fusion.1
  144.4 0.6 reduce-window.15
  145.1 0.7 convolution_minimum_fusion
  145.8 4.7 %fusion.12 = bf16[2048,512]{0,1:T(8,128)(2,1)} fusion(bf16[512,2048]{1,0:T(8,128)(2,1)S(1)} %bitcast.110, bf16[1,128,2048]{2,1,0:T(8,128)(2,1)S(1)} %copy-done, bf16[1,2048,128]{2,1,0:T(8,128)(2,1)} %param.28, f32[512,128]{1,0:T(8,128)S(1)} %convolution_minimum_fusion), kind=kOutput, calls=%fused_computation.20 | convolution fusion | flops 538509312 | bytes 5505024 | tf_op jit(solution)/shard_map/dot_general | solution.py:175
  150.5 3.2 %reshape_reshape.3 = bf16[8,2,128,512]{2,1,0,3:T(2,128)(2,1)S(1)} reshape(bf16[2048,512]{0,1:T(8,128)(2,1)} %fusion.12) | data formatting | bytes 4194304 | tf_op jit(solution)/shard_map/reshape;reshape | solution.py:61
  153.7 4.6 %copy.105 = bf16[8,2,128,512]{3,2,0,1:T(8,128)(2,1)} copy(bf16[8,2,128,512]{2,1,0,3:T(2,128)(2,1)S(1)} %reshape_reshape.3) | data formatting | bytes 4194304 | tf_op jit(solution)/shard_map/reshape;reshape | solution.py:61
  158.3 2.3 broadcast.142
  160.7 19.1 %fusion.23 = bf16[256,64]{0,1:T(8,128)(2,1)S(1)} fusion(f32[32,8,64,128]{3,2,1,0:T(8,128)S(1)} %bitcast.113, f32[32,8,64,128]{3,2,1,0:T(8,128)} %bitcast.112, f32[256,8192]{1,0:T(8,128)} %fusion, s32[256]{0:T(256)S(1)} %iota_add_fusion, bf16[8192,128]{0,1:T(8,128)(2,1)S(1)} %copy-done.1), kind=kOutput, calls=%fused_computation.39 | convolution fusion | flops 314589184 | bytes 26248192 | tf_op jit(solution)/shard_map/hts,shd->thd/dot_general | solution.py:99
  179.8 0.5 fusion.16
  180.3 1.2 copy.129
  181.5 7.8 %all-to-all-start = ((bf16[16,128,256]{1,2,0:T(8,128)(2,1)}), bf16[16,128,256]{1,2,0:T(8,128)(2,1)S(1)}, u32[]{:S(2)}, u32[]{:S(2)}) async-start(bf16[16,128,256]{1,2,0:T(8,128)(2,1)} %bitcast.105), calls=%async_computation | async-start | bytes 2097152 | tf_op jit(solution)/shard_map/all_to_all | solution.py:30
  189.4 24.4 %all-to-all-done = bf16[16,128,256]{1,2,0:T(8,128)(2,1)S(1)} async-done(((bf16[16,128,256]{1,2,0:T(8,128)(2,1)}), bf16[16,128,256]{1,2,0:T(8,128)(2,1)S(1)}, u32[]{:S(2)}, u32[]{:S(2)}) %all-to-all-start) | async-done | bytes 1048608 | tf_op jit(solution)/shard_map/all_to_all | solution.py:30
  214.0 0.6 broadcast_in_dim.31
  214.6 7.0 %all-to-all-start.1 = ((f32[16,1,256]{2,1,0:T(1,128)}), f32[16,1,256]{2,1,0:T(1,128)S(1)}, u32[]{:S(2)}, u32[]{:S(2)}) async-start(f32[16,1,256]{2,1,0:T(1,128)} %broadcast_in_dim.31), calls=%async_computation.1 | async-start | bytes 32768 | tf_op jit(solution)/shard_map/all_to_all | solution.py:36
  221.7 0.8 dynamic-slice_convert_fusion
  222.5 4.6 %all-to-all-done.1 = f32[16,1,256]{2,1,0:T(1,128)S(1)} async-done(((f32[16,1,256]{2,1,0:T(1,128)}), f32[16,1,256]{2,1,0:T(1,128)S(1)}, u32[]{:S(2)}, u32[]{:S(2)}) %all-to-all-start.1) | async-done | bytes 16416 | tf_op jit(solution)/shard_map/all_to_all | solution.py:36
  227.3 1.2 stack.2
  228.4 5.8 %all-to-all-start.2 = ((bf16[16,256,128]{2,1,0:T(8,128)(2,1)}), bf16[16,256,128]{2,1,0:T(8,128)(2,1)S(1)}, u32[]{:S(2)}, u32[]{:S(2)}) async-start(bf16[16,256,128]{2,1,0:T(8,128)(2,1)} %stack.2), calls=%async_computation.2 | async-start | bytes 2097152 | tf_op jit(solution)/shard_map/all_to_all | solution.py:150
  234.4 41.2 %reduce-scatter.5.cloned.1.call-done = bf16[1,128,512]{2,1,0:T(8,128)(2,1)} async-done(((bf16[8,128,512]{2,1,0:T(8,128)(2,1)}), bf16[1,128,512]{2,1,0:T(8,128)(2,1)}) %reduce-scatter.5.cloned.1.call-update) | async-done | bytes 131088 | tf_op jit(solution)/shard_map/reduce_scatter | solution.py:63
  275.6 1.7 copy.106
  277.3 10.7 %all-to-all-start.4 = ((bf16[128,32,16]{0,2,1:T(8,128)(2,1)}), bf16[128,32,16]{0,2,1:T(8,128)(2,1)S(1)}, u32[]{:S(2)}, u32[]{:S(2)}) async-start(bf16[128,32,16]{0,2,1:T(8,128)(2,1)} %bitcast.23), calls=%async_computation.6 | async-start | bytes 262144 | tf_op jit(solution)/shard_map/all_to_all | solution.py:185
  288.2 0.5 copy.98
  288.8 1.4 copy.108
  290.2 8.3 %all-to-all-done.4 = bf16[128,32,16]{0,2,1:T(8,128)(2,1)S(1)} async-done(((bf16[128,32,16]{0,2,1:T(8,128)(2,1)}), bf16[128,32,16]{0,2,1:T(8,128)(2,1)S(1)}, u32[]{:S(2)}, u32[]{:S(2)}) %all-to-all-start.4) | async-done | bytes 131104 | tf_op jit(solution)/shard_map/all_to_all | solution.py:185
  298.5 1.4 gather_fusion.1
  299.9 0.9 multiply_reduce_fusion
  (58 shorter events, 2.4 us)
Async XLA Ops:
  8.0 137.8 %copy-start = (bf16[1,128,2048]{2,1,0:T(8,128)(2,1)S(1)}, bf16[1,128,2048]{2,1,0:T(8,128)(2,1)}, u32[]{:S(2)}) copy-start(bf16[1,128,2048]{2,1,0:T(8,128)(2,1)} %param.29) | copy-start | bytes 1572868
  8.0 73.5 %all-gather.2.cloned.1.call-start = ((), (), s32[]{:S(2)}) async-start(), calls=%async_computation.7 | async-start | bytes 2359296 | tf_op jit(solution)/shard_map/all_gather | solution.py:18
  55.1 26.4 %copy-start.3 = (bf16[64,2048]{1,0:T(8,128)(2,1)S(1)}, bf16[64,2048]{1,0:T(8,128)(2,1)}, u32[]{:S(2)}) copy-start(bf16[64,2048]{1,0:T(8,128)(2,1)} %param.17) | copy-start | bytes 786436
  55.1 26.4 %copy-start.5 = (f32[1,8192]{1,0:T(1,128)S(1)}, f32[1,8192]{1,0:T(1,128)}, u32[]{:S(2)}) copy-start(f32[1,8192]{1,0:T(1,128)} %param.20) | copy-start | bytes 98308
  56.6 88.4 %all-to-all-start.3 = ((bf16[32,16,2048]{2,1,0:T(8,128)(2,1)}), bf16[32,16,2048]{2,1,0:T(8,128)(2,1)S(1)}, u32[]{:S(2)}, u32[]{:S(2)}) async-start(bf16[32,16,2048]{2,1,0:T(8,128)(2,1)} %broadcast_select_fusion), calls=%async_computation.3 | async-start | bytes 4194304 | tf_op jit(solution)/shard_map/all_to_all | solution.py:168
  67.8 159.3 %reduce-scatter.3.cloned.1.call-start = ((), (), s32[]{:S(2)}) async-start(), calls=%async_computation.8 | async-start | bytes 3145728 | tf_op jit(solution)/shard_map/reduce_scatter | solution.py:62
  134.6 10.5 %copy-start.2 = (bf16[1,2048,128]{2,1,0:T(8,128)(2,1)S(1)}, bf16[1,2048,128]{2,1,0:T(8,128)(2,1)}, u32[]{:S(2)}) copy-start(bf16[1,2048,128]{2,1,0:T(8,128)(2,1)} %param.27) | copy-start | bytes 1572868
  158.3 2.4 copy-start.1
  160.7 19.1 %copy-start.4 = (bf16[64,2048]{1,0:T(8,128)(2,1)S(1)}, bf16[64,2048]{1,0:T(8,128)(2,1)}, u32[]{:S(2)}) copy-start(bf16[64,2048]{1,0:T(8,128)(2,1)} %param.21) | copy-start | bytes 786436
  179.8 108.2 %copy-start.6 = (s32[96,4]{0,1:T(4,128)S(1)}, s32[96,4]{0,1:T(4,128)}, u32[]{:S(2)}) copy-start(s32[96,4]{0,1:T(4,128)} %param.25) | copy-start | bytes 4612
  179.8 108.3 %copy-start.7 = (f32[96,4]{0,1:T(4,128)S(1)}, f32[96,4]{0,1:T(4,128)}, u32[]{:S(2)}) copy-start(f32[96,4]{0,1:T(4,128)} %param.26) | copy-start | bytes 4612
  181.5 32.2 %all-to-all-start = ((bf16[16,128,256]{1,2,0:T(8,128)(2,1)}), bf16[16,128,256]{1,2,0:T(8,128)(2,1)S(1)}, u32[]{:S(2)}, u32[]{:S(2)}) async-start(bf16[16,128,256]{1,2,0:T(8,128)(2,1)} %bitcast.105), calls=%async_computation | async-start | bytes 2097152 | tf_op jit(solution)/shard_map/all_to_all | solution.py:30
  214.6 12.4 %all-to-all-start.1 = ((f32[16,1,256]{2,1,0:T(1,128)}), f32[16,1,256]{2,1,0:T(1,128)S(1)}, u32[]{:S(2)}, u32[]{:S(2)}) async-start(f32[16,1,256]{2,1,0:T(1,128)} %broadcast_in_dim.31), calls=%async_computation.1 | async-start | bytes 32768 | tf_op jit(solution)/shard_map/all_to_all | solution.py:36
  221.7 54.0 %reduce-scatter.5.cloned.1.call-start = ((), (), s32[]{:S(2)}) async-start(), calls=%async_computation.9 | async-start | bytes 1179648 | tf_op jit(solution)/shard_map/reduce_scatter | solution.py:63
  228.4 48.9 %all-to-all-start.2 = ((bf16[16,256,128]{2,1,0:T(8,128)(2,1)}), bf16[16,256,128]{2,1,0:T(8,128)(2,1)S(1)}, u32[]{:S(2)}, u32[]{:S(2)}) async-start(bf16[16,256,128]{2,1,0:T(8,128)(2,1)} %stack.2), calls=%async_computation.2 | async-start | bytes 2097152 | tf_op jit(solution)/shard_map/all_to_all | solution.py:150
  277.3 21.2 %all-to-all-start.4 = ((bf16[128,32,16]{0,2,1:T(8,128)(2,1)}), bf16[128,32,16]{0,2,1:T(8,128)(2,1)S(1)}, u32[]{:S(2)}, u32[]{:S(2)}) async-start(bf16[128,32,16]{0,2,1:T(8,128)(2,1)} %bitcast.23), calls=%async_computation.6 | async-start | bytes 262144 | tf_op jit(solution)/shard_map/all_to_all | solution.py:185
Sparse Core Ops, SparseCore 0:
  27.4 54.0 all-gather.1
Sparse Core Ops, SparseCore 1:
  158.4 18.2 reduce-scatter.2
  227.3 48.3 reduce-scatter.4
